TPU v7x, 1024 devices: a whole 4x8x16 slice. The times are simulated.
1024 devices in a mesh: sp: 128 (over z, y), tp: 8 (over x, core).
Axes of the slice: x: 4, y: 8, z: 16, core: 2. Of those that a mesh axis runs over, the one named last changes fastest.
Arguments:
- tokens: bfloat16 [98304, 2048], P('sp', 'tp'), may hold values from -18 to 18
- proj_weight: bfloat16 [2048, 1024], P(None, 'tp'), may hold values from -0.125 to 0.125
- gate_weight: bfloat16 [2048, 1024], P(None, 'tp'), may hold values from -0.125 to 0.125
- conv_weight: float32 [4, 1024], replicated, may hold values from -3 to 3
- recur_weight: bfloat16 [16, 64, 64], replicated, may hold values from -0.75 to 0.75
- input_weight: bfloat16 [16, 64, 64], replicated, may hold values from -0.75 to 0.75
- decay_param: float32 [1024], replicated, as said below
- out_grad: bfloat16 [98304, 1024], P('sp', 'tp'), may hold values from -6 to 6
Outputs:
- d_proj: bfloat16 [98304, 1024], P('sp', 'tp')
- d_gate: bfloat16 [98304, 1024], P('sp', 'tp')
- d_weight: float32 [2048, 1024], P('sp', 'tp')
Inputs may be any that keep to these rules, and one draw needn't show every extreme that they name: `decay_param`: every channel's decay parameter is at least 4; there is no fixed upper bound.
All inputs are finite; a program needn't handle non-finite values.
Results may differ from a plain program's by a relative error of at most 0.01.
Values may be sent and summed in bfloat16 or wider, within the bound.
A program may use at most 32 MiB of HBM per device.

v0:
```python
import jax
import jax.numpy as jnp
from jax import lax
from jax.sharding import Mesh
from jax.sharding import PartitionSpec as P

BLOCK = 64
SP = ("sp_0", "sp_1")


rate_scale = 8.0
scale_floor = 0.0001


def from_behind(value, axis, steps):
    count = lax.axis_size(axis)
    first, last = (max(0, -steps), min(count, count - steps))
    return lax.ppermute(value, axis, [(source, source + steps) for source in range(first, last)])


def filled_with(shard, identity):
    return jax.tree.map(
        lambda a, e: jnp.broadcast_to(jnp.asarray(e, a.dtype), a.shape), shard, identity
    )


def collected_together(shard, axis):
    leaves = jax.tree.leaves(shard)
    turns = sorted(range(len(leaves)), key=lambda k: -leaves[k].size)
    width = (1, *leaves[turns[0]].shape)[-1]
    lines = [
        jnp.pad(leaves[k].reshape(-1), (0, -leaves[k].size % width)).reshape(-1, width)
        for k in turns
    ]
    both, at, found = (lax.all_gather(jnp.concatenate(lines), axis), 0, {})
    for k, line in zip(turns, lines):
        share = both[:, at : at + len(line)].reshape(len(both), -1)
        found[k] = share[:, : leaves[k].size].reshape(-1, *leaves[k].shape)
        at += len(line)
    numbers = iter(range(len(leaves)))
    return jax.tree.map(lambda _: found[next(numbers)], shard)


def prefix_by_axis(shard, axes, combine, identity, reverse):
    before = start = filled_with(shard, identity)
    subtotal = shard
    for axis in reversed(axes):
        devices, position = (lax.axis_size(axis), lax.axis_index(axis))
        pieces = collected_together(subtotal, axis)
        inside, subtotal = (start, start)
        for k in reversed(range(devices)) if reverse else range(devices):
            passed = k > position if reverse else k < position
            subtotal = combine(subtotal, jax.tree.map(lambda part: part[k], pieces))
            inside = jax.tree.map(lambda new, old: jnp.where(passed, new, old), subtotal, inside)
        before = combine(inside, before)
    return before


def summed_rows(subtotal, axes):
    for axis in axes:
        subtotal = lax.psum_scatter(subtotal, axis, scatter_dimension=0, tiled=True)
    return subtotal


def combine(earlier, later):
    return (earlier[0] * later[0], later[0] * earlier[1] + later[1])


def block_map(values, weights, block_count):
    row_count = values.shape[0]
    shaped = values.reshape(row_count, block_count, BLOCK)
    result = jnp.einsum("tgi,gij->tgj", shaped, weights, preferred_element_type=jnp.float32)
    return result.reshape(row_count, block_count * BLOCK)


def block_back(values, weights, block_count):
    row_count = values.shape[0]
    shaped = values.reshape(row_count, block_count, BLOCK)
    result = jnp.einsum("tgj,gij->tgi", shaped, weights, preferred_element_type=jnp.float32)
    return result.reshape(row_count, block_count * BLOCK)


def per_device(
    tokens, proj_weight, gate_weight, conv_weight, recur_weight, input_weight, decay_param, out_grad
):
    tp_index = lax.axis_index("tp")
    row_count = tokens.shape[0]
    chan_width = proj_weight.shape[1]
    block_count = chan_width // BLOCK
    gathered = lax.all_gather(tokens, "tp", axis=1, tiled=True)
    projected = jnp.dot(gathered, proj_weight, preferred_element_type=jnp.float32).astype(
        jnp.bfloat16
    )
    gate_in = jnp.dot(gathered, gate_weight, preferred_element_type=jnp.float32).astype(
        jnp.bfloat16
    )
    conv_taps = lax.dynamic_slice_in_dim(conv_weight, tp_index * chan_width, chan_width, 1)
    decay_slice = lax.dynamic_slice_in_dim(decay_param, tp_index * chan_width, chan_width, 0)
    w_recur = lax.dynamic_slice_in_dim(recur_weight, tp_index * block_count, block_count, 0)
    w_input = lax.dynamic_slice_in_dim(input_weight, tp_index * block_count, block_count, 0)
    prior_rows = from_behind(projected[row_count - 3 :], SP, 1)
    padded = jnp.concatenate([prior_rows, projected], axis=0).astype(jnp.float32)
    total = conv_taps[0] * padded[3 : 3 + row_count]
    for offset in range(1, 4):
        total = total + conv_taps[offset] * padded[3 - offset : 3 - offset + row_count]
    conv_out = total.astype(jnp.bfloat16)
    conv_float = conv_out.astype(jnp.float32)
    recur_open = jax.nn.sigmoid(block_map(conv_out, w_recur, block_count))
    input_open = jax.nn.sigmoid(block_map(conv_out, w_input, block_count))
    log_slope = rate_scale * jax.nn.log_sigmoid(decay_slice)
    log_decay = log_slope * recur_open
    decay_rate = jnp.exp(log_decay)
    input_scale = jnp.sqrt(scale_floor - jnp.expm1(2.0 * log_decay))
    gated_input = input_open * conv_float
    drive = input_scale * gated_input
    cum_decay, local_states = lax.associative_scan(combine, (decay_rate, drive), axis=0)
    gelu_gate, gelu_back = jax.vjp(jax.nn.gelu, gate_in.astype(jnp.float32))
    cotangent = out_grad.astype(jnp.float32)
    drive_grad = cotangent * gelu_gate
    shifted = jnp.concatenate([decay_rate[1:], jnp.ones((1, chan_width), jnp.float32)], axis=0)
    cum_after, local_grad = lax.associative_scan(
        combine, (shifted, drive_grad), reverse=True, axis=0
    )
    span_decay = cum_decay[-1]
    span_state = local_states[-1]
    span_grad = decay_rate[0] * local_grad[0]
    ones_row = jnp.ones((chan_width,), jnp.float32)
    zeros_row = jnp.zeros((chan_width,), jnp.float32)
    _, carry_state = prefix_by_axis(
        (span_decay, span_state), SP, combine, (ones_row, zeros_row), False
    )
    _, carry_grad = prefix_by_axis(
        (span_decay, span_grad), SP, combine, (ones_row, zeros_row), True
    )
    states = local_states + cum_decay * carry_state
    previous = jnp.concatenate([carry_state[None], states[:-1]], axis=0)
    d_gate = gelu_back(cotangent * states)[0].astype(jnp.bfloat16)
    state_grad = local_grad + cum_after * carry_grad
    d_log_decay = state_grad * (
        decay_rate * previous - gated_input * decay_rate * decay_rate / input_scale
    )
    d_recur_pre = (d_log_decay * log_slope * recur_open * (1.0 - recur_open)).astype(jnp.bfloat16)
    d_input_pre = (state_grad * input_scale * conv_float * input_open * (1.0 - input_open)).astype(
        jnp.bfloat16
    )
    d_conv = state_grad * input_scale * input_open
    d_conv = d_conv + block_back(d_recur_pre, w_recur, block_count)
    d_conv = d_conv + block_back(d_input_pre, w_input, block_count)
    next_rows = from_behind(d_conv[:3], SP, -1)
    extended = jnp.concatenate([d_conv, next_rows], axis=0)
    grad_sum = conv_taps[0] * extended[0:row_count]
    for offset in range(1, 4):
        grad_sum = grad_sum + conv_taps[offset] * extended[offset : offset + row_count]
    d_proj = grad_sum.astype(jnp.bfloat16)
    d_weight = summed_rows(
        lax.dot_general(
            gathered, d_proj, (((0,), (0,)), ((), ())), preferred_element_type=jnp.float32
        ),
        SP,
    )
    return (d_proj, d_gate, d_weight)


def solution(mesh):
    split = Mesh(mesh.devices.reshape(16, 8, mesh.shape["tp"]), ("sp_0", "sp_1", "tp"))
    placed = (P(SP, "tp"), P(None, "tp"), P(None, "tp"), P(), P(), P(), P(), P(SP, "tp"))
    return jax.shard_map(
        per_device,
        mesh=split,
        in_specs=placed,
        out_specs=(P(SP, "tp"), P(SP, "tp"), P(SP, "tp")),
        check_vma=False,
    )
```

profile of v0, /device:TPU:1, one launch (start us, length us, event | category | flops | bytes accessed | tf_op | source)
XLA Modules:
  0.0 323.1 jit_solution(10317154471683664710)
XLA Ops:
  8.0 0.8 fusion.95
  9.5 52.2 %all-gather.10.cloned.1.call-done = bf16[768,2048]{1,0:T(8,128)(2,1)} async-done(((bf16[768,256]{1,0:T(8,128)(2,1)}), bf16[768,2048]{1,0:T(8,128)(2,1)}) %all-gather.10.cloned.1.call-update) | async-done | bytes 3145744 | tf_op jit(solution)/shard_map/all_gather | solution.py:90
  61.8 3.0 convolution_convert_fusion
  64.7 2.8 collective-permute-start
  68.7 1.1 fusion.2
  69.9 1.1 fusion.5
  72.7 0.7 slice.1200
  73.5 1.0 multiply_add_fusion.2
  77.2 0.9 pad.273
  79.7 1.0 pad.293
  80.7 2.5 pad.275
  84.0 12.9 %all-gather.6 = f32[8,2,128]{2,1,0:T(2,128)S(1)} all-gather(f32[1,2,128]{2,1,0:T(2,128)S(1)} %fusion.58), channel_id=4, replica_groups=mesh['sp_0'=16,'sp_1'=8,'tp'=8] {'sp_1'}, dimensions={0}, use_global_device_ids=true | all-gather | bytes 9216 | tf_op jit(solution)/shard_map/all_gather | solution.py:35
  96.9 24.2 %all-gather.7 = f32[16,2,128]{2,1,0:T(2,128)S(1)} all-gather(f32[1,2,128]{2,1,0:T(2,128)S(1)} %maximum_bitcast_fusion.1), channel_id=5, replica_groups=mesh['sp_0'=16,'sp_1'=8,'tp'=8] {'sp_0'}, dimensions={0}, use_global_device_ids=true | all-gather | bytes 17408 | tf_op jit(solution)/shard_map/all_gather | solution.py:35
  121.1 4.2 %fusion.16 = (bf16[768,128]{1,0:T(8,128)(2,1)}, f32[768,128]{1,0:T(8,128)}, f32[768,128]{1,0:T(8,128)S(1)}) fusion(bf16[768,128]{1,0:T(8,128)(2,1)} %param.15, f32[128]{0:T(128)S(1)} %fusion.68, f32[768,128]{1,0:T(8,128)S(1)} %pad.274, f32[768,128]{1,0:T(8,128)} %pad.275, f32[768,128]{1,0:T(8,128)S(1)} %pad.292, f32[768,128]{1,0:T(8,128)} %copy-done.3, ...), kind=kOutput, calls=%fused_computation.30 | convolution fusion | flops 405602304 | bytes 6423040 | tf_op jit(solution)/shard_map/dot_general | solution.py:94
  125.8 0.8 slice.1111
  126.6 0.7 slice.1109
  127.6 1.7 slice.1112
  130.6 1.8 slice.1110
  134.2 0.9 pad.237
  135.8 0.7 add.1080
  136.7 1.0 pad.239
  137.8 11.9 %all-gather.4 = f32[8,2,128]{2,1,0:T(2,128)S(1)} all-gather(f32[1,2,128]{2,1,0:T(2,128)S(1)} %fusion.57), channel_id=2, replica_groups=mesh['sp_0'=16,'sp_1'=8,'tp'=8] {'sp_1'}, dimensions={0}, use_global_device_ids=true | all-gather | bytes 9216 | tf_op jit(solution)/shard_map/all_gather | solution.py:35
  149.9 20.5 %all-gather.5 = f32[16,2,128]{2,1,0:T(2,128)S(1)} all-gather(f32[1,2,128]{2,1,0:T(2,128)S(1)} %maximum_bitcast_fusion), channel_id=3, replica_groups=mesh['sp_0'=16,'sp_1'=8,'tp'=8] {'sp_0'}, dimensions={0}, use_global_device_ids=true | all-gather | bytes 17408 | tf_op jit(solution)/shard_map/all_gather | solution.py:35
  170.7 1.7 fusion.9
  172.6 0.9 fusion.46
  173.8 0.9 fusion.49
  175.1 1.3 collective-permute-start.1
  176.4 3.3 %collective-permute-done.1 = f32[3,128]{1,0:T(4,128)S(1)} collective-permute-done((f32[3,128]{1,0:T(4,128)S(1)}, f32[3,128]{1,0:T(4,128)S(1)}, u32[]{:S(2)}, u32[]{:S(2)}) %collective-permute-start.1) | collective-permute-done | bytes 1568 | tf_op jit(solution)/shard_map/ppermute | solution.py:18
  179.9 3.5 %convolution_bitcast_fusion = f32[2048,128]{0,1:T(8,128)} fusion(bf16[768,128]{1,0:T(8,128)(2,1)S(1)} %fusion.21, bf16[768,2048]{1,0:T(8,128)(2,1)} %all-gather.10.cloned.1.call-done), kind=kOutput, calls=%fused_computation | convolution fusion | flops 402653184 | bytes 4390912 | tf_op jit(solution)/shard_map/dot_general | solution.py:156
  183.5 83.2 %reduce-scatter.5.cloned.1.call-done = f32[128,128]{0,1:T(8,128)} async-done(((f32[2048,128]{0,1:T(8,128)}), f32[128,128]{0,1:T(8,128)}) %reduce-scatter.5.cloned.1.call-update) | async-done | bytes 65552 | tf_op jit(solution)/shard_map/reduce_scatter | solution.py:61
  266.7 1.6 copy.60
  268.3 48.3 %reduce-scatter.7.cloned.1.call-done = f32[16,128]{1,0:T(8,128)} async-done(((f32[128,128]{1,0:T(8,128)}), f32[16,128]{1,0:T(8,128)}) %reduce-scatter.7.cloned.1.call-update) | async-done | bytes 8208
  (341 shorter events, 14.3 us)
Async XLA Ops:
  7.2 114.0 %copy-start = (bf16[2048,128]{1,0:T(8,128)(2,1)S(1)}, bf16[2048,128]{1,0:T(8,128)(2,1)}, u32[]{:S(2)}) copy-start(bf16[2048,128]{1,0:T(8,128)(2,1)} %param.10) | copy-start | bytes 1572868
  7.2 54.6 %all-gather.10.cloned.1.call-start = ((), (), s32[]{:S(2)}) async-start(), calls=%async_computation.2 | async-start | bytes 3538944 | tf_op jit(solution)/shard_map/all_gather | solution.py:90
  7.9 258.8 %reduce-scatter.5.cloned.1.call-start = ((), (), s32[]{:S(2)}) async-start(), calls=%async_computation.3 | async-start | bytes 1114112 | tf_op jit(solution)/shard_map/reduce_scatter | solution.py:61
  64.7 3.5 %collective-permute-start = (bf16[3,128]{1,0:T(4,128)(2,1)S(1)}, bf16[3,128]{1,0:T(4,128)(2,1)S(1)}, u32[]{:S(2)}, u32[]{:S(2)}) collective-permute-start(bf16[3,128]{1,0:T(4,128)(2,1)S(1)} %slice.1390), channel_id=1, source_target_pairs={{0,8},{8,16},{16,24},{24,32},{32,40},{40,48},{48,56},{56,64},{64,7... | collective-permute-start | bytes 2312 | tf_op jit(solution)/shard_map/ppermute | solution.py:18
  80.7 40.4 %copy-start.3 = (f32[768,128]{1,0:T(8,128)}, f32[768,128]{1,0:T(8,128)S(1)}, u32[]{:S(2)}) copy-start(f32[768,128]{1,0:T(8,128)S(1)} %pad.293) | copy-start | bytes 1179652
  136.6 33.8 %copy-start.2 = (f32[384,128]{1,0:T(8,128)S(1)}, f32[384,128]{1,0:T(8,128)}, u32[]{:S(2)}) copy-start(f32[384,128]{1,0:T(8,128)} %add.1080) | copy-start | bytes 589828
  175.1 4.6 %collective-permute-start.1 = (f32[3,128]{1,0:T(4,128)S(1)}, f32[3,128]{1,0:T(4,128)S(1)}, u32[]{:S(2)}, u32[]{:S(2)}) collective-permute-start(f32[3,128]{1,0:T(4,128)S(1)} %slice.1573), channel_id=1, source_target_pairs={{8,0},{16,8},{24,16},{32,24},{40,32},{48,40},{56,48},{64,56},{72,6... | collective-permute-start | bytes 4616 | tf_op jit(solution)/shard_map/ppermute | solution.py:18
  179.9 136.7 %copy-start.1 = (bf16[768,128]{1,0:T(8,128)(2,1)}, bf16[768,128]{1,0:T(8,128)(2,1)S(1)}, u32[]{:S(2)}) copy-start(bf16[768,128]{1,0:T(8,128)(2,1)S(1)} %fusion.21) | copy-start | bytes 589828
  183.5 133.1 %reduce-scatter.7.cloned.1.call-start = ((), (), s32[]{:S(2)}) async-start(), calls=%async_computation.4 | async-start | bytes 73728
Sparse Core Ops, SparseCore 0:
  10.7 51.0 all-gather.9
  183.6 83.0 reduce-scatter.4
  270.6 45.8 reduce-scatter.6
where the time goes:
time: 329 us; the launch traced here: 323 us
  waiting for transfers between devices  188 us (57%)
  blocking collectives  69.3 us (21%)
  local copies, waits for them, and re-layouts  20 us (6%)
  between operations  15.7 us (5%)
  matrix products  14.7 us (4%)
  other arithmetic  10.6 us (3%)
  starting transfers between devices  4.23 us (1%)
    reduce_scatter x1, waiting for transfers between devices, summed_rows(): subtotal = lax.psum_scatter(subtotal, axis, scatter_dimension=0, tiled=True)  83.2 us
    all_gather x4, blocking collectives, collected_together(): both, at, found = (lax.all_gather(jnp.concatenate(lines), axis), 0, {})  69.3 us
    all_gather x1, waiting for transfers between devices, per_device(): gathered = lax.all_gather(tokens, 'tp', axis=1, tiled=True)  52.2 us
    unnamed x4, waiting for transfers between devices  49 us
    slice x69, local copies, waits for them, and re-layouts, per_device(): lax.associative_scan(combine, (shifted, drive_grad), reverse=True, axis=0)  6.62 us
  transfers between devices with their start and end apart: 5, of which 5 were waited for; matrix products, arithmetic and copies ran while one was open for 0% of the time, Pallas kernels for 0%

commit v1 on v0

v1 whole, which is shorter than its diff:
```python
import functools

import jax
import jax.numpy as jnp
from jax import lax
from jax.experimental import pallas as pl
from jax.experimental.pallas import tpu as pltpu
from jax.sharding import Mesh
from jax.sharding import PartitionSpec as P

MESH = pl.DeviceIdType.MESH
F32 = jnp.float32
BF16 = jnp.bfloat16
BLOCK = 64
HALO = 16
LANES = 128
RATE = 8.0
FLOOR = 0.0001
GELU_A = 0.7978845608028654
GELU_B = 0.044715
CHUNK = 80


def small_expm1(x):
    p = 1.0 / 5040.0
    for c in (1.0 / 720.0, 1.0 / 120.0, 1.0 / 24.0, 1.0 / 6.0, 0.5, 1.0):
        p = p * x + c
    return p * x


def small_log1p(u):
    p = -1.0 / 6.0
    for c in (1.0 / 5.0, -1.0 / 4.0, 1.0 / 3.0, -0.5, 1.0):
        p = p * u + c
    return p * u


def kernel(
    dims, tok, pw, gw, cw, rw, iw, dp, og, dproj, dgate, dweight,
    G, WP, WG, OG, RW, IW, ACC, PJ, CV, PRE, A, B, DG, RO, IO, SC, DGL, HP, PP, YN, QN, DR, DC,
    SUM, RYC, SUMZ, RZC, CF, CB, WS, RY, VZ, RZ,
    lsem, hps, hpr, hns, hnr, ogs, ags, agr, ycs, ycr, zcs, zcr, rys, ryr, rzs, rzr,
):
    NZ, NY, NX, rows = dims
    R = rows + 2 * HALO
    SEG = R // 8
    nch = R // CHUNK
    z, y, x, c = (lax.axis_index(n) for n in ("z", "y", "x", "c"))
    sp = z * NY + y
    nsp = NZ * NY
    tp = x * 2 + c
    nxt, prv = lax.rem(sp + 1, nsp), lax.rem(sp + nsp - 1, nsp)
    nz, ny = nxt // NY, lax.rem(nxt, NY)
    pz, py = prv // NY, lax.rem(prv, NY)
    left, right, opp = lax.rem(x + NX - 1, NX), lax.rem(x + 1, NX), lax.rem(x + 2, NX)

    loads = [
        pltpu.make_async_copy(tok.at[:, pl.ds(h * LANES, LANES)], G.at[2 * tp + h, pl.ds(HALO, rows)], lsem.at[h])
        for h in range(2)
    ]
    loads += [
        pltpu.make_async_copy(pw, WP, lsem.at[2]),
        pltpu.make_async_copy(gw, WG, lsem.at[3]),
        pltpu.make_async_copy(og, OG.at[pl.ds(HALO, rows)], lsem.at[4]),
        pltpu.make_async_copy(rw.at[pl.ds(2 * tp, 2)], RW, lsem.at[5]),
        pltpu.make_async_copy(iw.at[pl.ds(2 * tp, 2)], IW, lsem.at[6]),
    ]
    for copy in loads:
        copy.start()

    barrier = pltpu.get_barrier_semaphore()

    def greet(**where):
        pl.semaphore_signal(barrier, inc=1, device_id=where, device_id_type=MESH)

    greet(c=1 - c)
    greet(x=left)
    greet(x=right)
    for k in range(NX):
        for d in range(2):
            greet(z=nz, y=ny, x=k, c=d)
            greet(z=pz, y=py, x=k, c=d)
    for d in range(1, NY):
        greet(y=lax.rem(y + d, NY))
    for d in range(1, NZ):
        greet(z=lax.rem(z + d, NZ))
    pl.semaphore_wait(barrier, 3 + 4 * NX + NY - 1 + NZ - 1)

    pending = []

    def send(src, dst, ssem, rsem, **where):
        copy = pltpu.make_async_remote_copy(
            src_ref=src, dst_ref=dst, send_sem=ssem, recv_sem=rsem, device_id=where, device_id_type=MESH
        )
        copy.start()
        pending.append(copy)

    def arrived(dst, ssem, rsem, **where):
        pltpu.make_async_remote_copy(
            src_ref=dst, dst_ref=dst, send_sem=ssem, recv_sem=rsem, device_id=where, device_id_type=MESH
        ).wait_recv()

    loads[0].wait()
    loads[1].wait()
    mine = 2 * tp
    main = pl.ds(HALO, rows)
    for k in range(NX):
        for d in range(2):
            n = 2 * k + d
            send(G.at[pl.ds(mine, 2), pl.ds(rows, HALO)], G.at[pl.ds(mine, 2), pl.ds(0, HALO)],
                 hps.at[n], hpr.at[tp], z=nz, y=ny, x=k, c=d)
            send(G.at[pl.ds(mine, 2), pl.ds(HALO, HALO)], G.at[pl.ds(mine, 2), pl.ds(HALO + rows, HALO)],
                 hns.at[n], hnr.at[tp], z=pz, y=py, x=k, c=d)

    def piece(xx, cc, h):
        return 4 * xx + 2 * cc + h

    def give(i, sem, **where):
        send(G.at[i, main], G.at[i, main], ags.at[sem], agr.at[sem], **where)

    def got(i, sem):
        arrived(G.at[i, main], ags.at[sem], agr.at[sem], c=1 - c)

    p0, p1 = piece(x, c, 0), piece(x, c, 1)
    give(p0, 0, x=right)
    give(p1, 1, x=left)
    give(p1, 2, x=right)
    give(p0, 3, x=left)
    give(p0, 6, c=1 - c)
    give(p1, 7, c=1 - c)
    loads[4].wait()
    send(OG.at[pl.ds(HALO, HALO)], OG.at[pl.ds(HALO + rows, HALO)], ogs.at[0], ogs.at[1], z=pz, y=py)
    for k in (2, 3, 5, 6):
        loads[k].wait()

    OG[pl.ds(0, HALO), :] = jnp.zeros((HALO, LANES), BF16)
    PJ[pl.ds(0, 8), :] = jnp.zeros((8, LANES), F32)
    DC[pl.ds(R, 8), :] = jnp.zeros((8, LANES), F32)
    slope = -RATE * small_log1p(jnp.exp(-dp[pl.ds(tp, 1), :]))
    taps = [cw[pl.ds(k, 1), pl.ds(pl.multiple_of(tp * LANES, LANES), LANES)] for k in range(4)]
    zero = jnp.zeros((BLOCK, BLOCK), BF16)
    gates = jnp.concatenate(
        [
            jnp.concatenate([RW[0], zero, IW[0], zero], axis=1),
            jnp.concatenate([zero, RW[1], zero, IW[1]], axis=1),
        ],
        axis=0,
    )

    for n in range(2 * NX):
        arrived(G.at[pl.ds(2 * n, 2), pl.ds(0, HALO)], hps.at[n], hpr.at[n], c=1 - c)
        arrived(G.at[pl.ds(2 * n, 2), pl.ds(HALO + rows, HALO)], hns.at[n], hnr.at[n], c=1 - c)
    arrived(OG.at[pl.ds(HALO + rows, HALO)], ogs.at[0], ogs.at[1], c=1 - c)

    @pl.when(sp == 0)
    def _():
        G[:, pl.ds(0, HALO), :] = jnp.zeros((4 * NX, HALO, LANES), BF16)

    @pl.when(sp == nsp - 1)
    def _():
        G[:, pl.ds(HALO + rows, HALO), :] = jnp.zeros((4 * NX, HALO, LANES), BF16)
        OG[pl.ds(HALO + rows, HALO), :] = jnp.zeros((HALO, LANES), BF16)

    def multiply(i0, i1, first=False):
        def half(i):
            at = pl.ds(pl.multiple_of(i * LANES, LANES), LANES)
            return jnp.concatenate([WP[at, :], WG[at, :]], axis=1)

        rhs = jnp.concatenate([half(i0), half(i1)], axis=0)
        lhs = jnp.concatenate([G[i0], G[i1]], axis=1)
        out = jnp.dot(lhs, rhs, preferred_element_type=F32)
        if first:
            ACC[...] = out
        else:
            ACC[...] += out

    multiply(p0, p1, True)
    got(piece(x, 1 - c, 0), 6)
    got(piece(x, 1 - c, 1), 7)
    multiply(piece(x, 1 - c, 0), piece(x, 1 - c, 1))

    l0, l1 = piece(left, c, 0), piece(left, c, 1)
    r0, r1 = piece(right, c, 0), piece(right, c, 1)
    o0, o1 = piece(opp, c, 0), piece(opp, c, 1)
    got(l0, 0)
    give(l0, 4, x=right)
    give(l0, 8, c=1 - c)
    got(r1, 1)
    give(r1, 5, x=left)
    give(r1, 9, c=1 - c)
    multiply(l0, r1)
    got(piece(left, 1 - c, 0), 8)
    got(piece(right, 1 - c, 1), 9)
    multiply(piece(left, 1 - c, 0), piece(right, 1 - c, 1))
    got(l1, 2)
    give(l1, 10, c=1 - c)
    got(r0, 3)
    give(r0, 11, c=1 - c)
    multiply(l1, r0)
    got(piece(left, 1 - c, 1), 10)
    got(piece(right, 1 - c, 0), 11)
    multiply(piece(left, 1 - c, 1), piece(right, 1 - c, 0))
    got(o0, 4)
    give(o0, 12, c=1 - c)
    got(o1, 5)
    give(o1, 13, c=1 - c)
    multiply(o0, o1)
    got(piece(opp, 1 - c, 0), 12)
    got(piece(opp, 1 - c, 1), 13)
    multiply(piece(opp, 1 - c, 0), piece(opp, 1 - c, 1))

    PJ[pl.ds(8, R), :] = ACC[:, pl.ds(0, LANES)].astype(BF16).astype(F32)

    def convolve(i, _):
        base = pl.multiple_of(i * CHUNK, CHUNK)
        part = PJ[pl.ds(base, CHUNK + 8), :]
        total = taps[0] * part[8:]
        for k in range(1, 4):
            total = total + taps[k] * pltpu.roll(part, k, 0)[8:]
        CV[pl.ds(base, CHUNK), :] = total.astype(BF16)
        return 0

    lax.fori_loop(0, nch, convolve, 0)
    PRE[...] = jnp.dot(CV[...], gates, preferred_element_type=F32)

    def local(i, _):
        base = pl.multiple_of(i * CHUNK, CHUNK)
        at = pl.ds(base, CHUNK)
        ro = jax.nn.sigmoid(PRE[at, pl.ds(0, LANES)])
        io = jax.nn.sigmoid(PRE[at, pl.ds(LANES, LANES)])
        conv = CV[at, :].astype(F32)
        e = small_expm1(slope * ro)
        sc = jnp.sqrt(FLOOR - e * (2.0 + e))
        row = lax.broadcasted_iota(jnp.int32, (CHUNK, LANES), 0) + base
        own = row >= HALO
        A[at, :] = jnp.where(own, 1.0 + e, 1.0)
        B[at, :] = jnp.where(own, sc * (io * conv), 0.0)
        RO[at, :] = ro
        IO[at, :] = io
        SC[at, :] = sc
        q = ACC[at, pl.ds(LANES, LANES)].astype(BF16).astype(F32)
        cot = OG[at, :].astype(F32)
        t = jnp.tanh(GELU_A * (q + GELU_B * (q * q * q)))
        cdf = 0.5 * (1.0 + t)
        DG[at, :] = cot * (q * cdf)
        DGL[at, :] = cot * (cdf + 0.5 * q * (1.0 - t * t) * (GELU_A * (1.0 + 3.0 * GELU_B * (q * q))))
        return 0

    lax.fori_loop(0, nch, local, 0)

    STEP = 10

    def scan(i, carry):
        h, p, yb, q = carry
        for k in range(STEP):
            v = i * STEP + k
            fw, bw = pl.ds(v, 8, stride=SEG), pl.ds(SEG - 1 - v, 8, stride=SEG)
            a, b = A[fw, :], B[fw, :]
            HP[fw, :] = h
            PP[fw, :] = p
            h = a * h + b
            p = p * a
            a, g = A[bw, :], DG[bw, :]
            YN[bw, :] = yb
            QN[bw, :] = q
            yb = a * (g + yb)
            q = q * a
        return h, p, yb, q

    one, nil = jnp.ones((8, LANES), F32), jnp.zeros((8, LANES), F32)
    h, p, yb, q = lax.fori_loop(0, SEG // STEP, scan, (nil, one, nil, one))

    fa, fs, s_of, a_of = one[0:1], nil[0:1], [], []
    for k in range(8):
        s_of.append(fs)
        a_of.append(fa)
        fs = h[k : k + 1] + p[k : k + 1] * fs
        fa = fa * p[k : k + 1]
    ba, bs, t_of, c_of = one[0:1], nil[0:1], [None] * 8, [None] * 8
    for k in reversed(range(8)):
        t_of[k] = bs
        c_of[k] = ba
        bs = yb[k : k + 1] + q[k : k + 1] * bs
        ba = ba * q[k : k + 1]
    last, lead = HALO + rows - 1, 2 * HALO
    ls, fsg = last // SEG, lead // SEG
    la, lb = A[pl.ds(last, 1), :], B[pl.ds(last, 1), :]
    lp = PP[pl.ds(last, 1), :]
    out_a = la * lp * a_of[ls]
    out_s = la * (HP[pl.ds(last, 1), :] + lp * s_of[ls]) + lb
    ga, gg = A[pl.ds(lead, 1), :], DG[pl.ds(lead, 1), :]
    gq = QN[pl.ds(lead, 1), :]
    out_c = ga * gq * c_of[fsg]
    out_l = ga * (gg + YN[pl.ds(lead, 1), :] + gq * t_of[fsg])

    def put(ref, values):
        for k, value in enumerate(values):
            ref[pl.ds(k, 1), :] = value

    SUM[...] = nil
    put(SUM, (out_a, out_s, out_c, out_l))
    for d in range(1, NY):
        send(SUM, RYC.at[y], ycs.at[d], ycr.at[y], y=lax.rem(y + d, NY))
    RYC[y] = SUM[...]
    for d in range(1, NY):
        k = lax.rem(y + d, NY)
        arrived(RYC.at[k], ycs.at[d], ycr.at[k], c=1 - c)

    def compose(ref, count, place):
        fa, fs, fai, fsi = one[0:1], nil[0:1], one[0:1], nil[0:1]
        for k in range(count):
            a, s = ref[k, pl.ds(0, 1), :], ref[k, pl.ds(1, 1), :]
            fa, fs = fa * a, a * fs + s
            before = k < place
            fai, fsi = jnp.where(before, fa, fai), jnp.where(before, fs, fsi)
        ba, bs, bai, bsi = one[0:1], nil[0:1], one[0:1], nil[0:1]
        for k in reversed(range(count)):
            a, s = ref[k, pl.ds(2, 1), :], ref[k, pl.ds(3, 1), :]
            ba, bs = ba * a, a * bs + s
            after = k > place
            bai, bsi = jnp.where(after, ba, bai), jnp.where(after, bs, bsi)
        return (fa, fs, ba, bs), (fai, fsi, bai, bsi)

    total, inside = compose(RYC, NY, y)
    SUMZ[...] = nil
    put(SUMZ, total)
    for d in range(1, NZ):
        send(SUMZ, RZC.at[z], zcs.at[d], zcr.at[z], z=lax.rem(z + d, NZ))
    RZC[z] = SUMZ[...]
    for d in range(1, NZ):
        k = lax.rem(z + d, NZ)
        arrived(RZC.at[k], zcs.at[d], zcr.at[k], c=1 - c)
    _, outer = compose(RZC, NZ, z)
    carry_s = inside[1] + inside[0] * outer[1]
    carry_g = inside[3] + inside[2] * outer[3]
    put(CF, [s_of[k] + a_of[k] * carry_s for k in range(8)])
    put(CB, [t_of[k] + c_of[k] * carry_g for k in range(8)])
    cf, cb = CF[...], CB[...]

    def finish(i, _):
        for k in range(STEP):
            at = pl.ds(i * STEP + k, 8, stride=SEG)
            HP[at, :] = HP[at, :] + PP[at, :] * cf
            YN[at, :] = YN[at, :] + QN[at, :] * cb
        return 0

    lax.fori_loop(0, SEG // STEP, finish, 0)

    def gradients(i, _):
        base = pl.multiple_of(i * CHUNK, CHUNK)
        at = pl.ds(base, CHUNK)
        a, ro, io, sc = A[at, :], RO[at, :], IO[at, :], SC[at, :]
        conv = CV[at, :].astype(F32)
        decayed = a * HP[at, :]
        grad = DG[at, :] + YN[at, :]
        gated = io * conv
        DGL[at, :] = DGL[at, :] * (decayed + B[at, :])
        d_log = grad * (decayed - gated * a * a / sc)
        DR[at, pl.ds(0, LANES)] = (d_log * slope * ro * (1.0 - ro)).astype(BF16)
        gs = grad * sc
        DR[at, pl.ds(LANES, LANES)] = (gs * conv * io * (1.0 - io)).astype(BF16)
        DC[at, :] = gs * io
        return 0

    lax.fori_loop(0, nch, gradients, 0)
    dgate[...] = DGL[pl.ds(HALO, rows), :].astype(BF16)
    DC[pl.ds(0, R), :] += lax.dot_general(DR[...], gates, (((1,), (1,)), ((), ())), preferred_element_type=F32)

    WIDE = 96

    def unconvolve(i, _):
        base = pl.multiple_of(i * WIDE, WIDE)
        part = DC[pl.ds(base + HALO, WIDE + 8), :]
        total = taps[0] * part[:WIDE]
        for k in range(1, 4):
            total = total + taps[k] * pltpu.roll(part, WIDE + 8 - k, 0)[:WIDE]
        dproj[pl.ds(base, WIDE), :] = total.astype(BF16)
        return 0

    lax.fori_loop(0, rows // WIDE, unconvolve, 0)

    grad = dproj[...]
    share = LANES // NY
    per = NZ // 4
    for g in range(4):
        for i in range(g * per, (g + 1) * per):
            part = lax.dot_general(G[i, main, :], grad, (((0,), (0,)), ((), ())), preferred_element_type=F32)
            WS[:, i] = part.astype(BF16).reshape(NY, share, LANES)
        for d in range(1, NY):
            k = lax.rem(y + d, NY)
            send(WS.at[k, pl.ds(g * per, per)], RY.at[y, pl.ds(g * per, per)], rys.at[g, d], ryr.at[g, y], y=k)
    for g in range(4):
        total = WS[y, pl.ds(g * per, per)].astype(F32)
        for d in range(1, NY):
            k = lax.rem(y + d, NY)
            arrived(RY.at[k, pl.ds(g * per, per)], rys.at[g, d], ryr.at[g, k], c=1 - c)
            total = total + RY[k, pl.ds(g * per, per)].astype(F32)
        VZ[pl.ds(g * per, per)] = total.astype(BF16)
    for d in range(1, NZ):
        k = lax.rem(z + d, NZ)
        send(VZ.at[k], RZ.at[z], rzs.at[d], rzr.at[z], z=k)
    total = VZ[z].astype(F32)
    for d in range(1, NZ):
        k = lax.rem(z + d, NZ)
        arrived(RZ.at[k], rzs.at[d], rzr.at[k], c=1 - c)
        total = total + RZ[k].astype(F32)
    dweight[...] = total
    for copy in pending:
        copy.wait_send()


def per_device(dims, tokens, proj_weight, gate_weight, conv_weight, recur_weight, input_weight, decay_param, out_grad):
    NZ, NY, NX, rows = dims
    R = rows + 2 * HALO
    share = LANES // NY
    vmem = pltpu.VMEM
    dma = pltpu.SemaphoreType.DMA
    flat = [vmem((R, LANES), F32)] * 11
    anywhere, inside = pl.BlockSpec(memory_space=pl.ANY), pl.BlockSpec(memory_space=pltpu.VMEM)
    return pl.pallas_call(
        functools.partial(kernel, dims),
        out_shape=(
            jax.ShapeDtypeStruct((rows, LANES), BF16),
            jax.ShapeDtypeStruct((rows, LANES), BF16),
            jax.ShapeDtypeStruct((share, LANES), F32),
        ),
        in_specs=[anywhere, anywhere, anywhere, inside, anywhere, anywhere, inside, anywhere],
        out_specs=(inside, inside, inside),
        scratch_shapes=[
            vmem((4 * NX, R, LANES), BF16),
            vmem(proj_weight.shape, BF16),
            vmem(gate_weight.shape, BF16),
            vmem((R, LANES), BF16),
            vmem((2, BLOCK, BLOCK), BF16),
            vmem((2, BLOCK, BLOCK), BF16),
            vmem((R, 2 * LANES), F32),
            vmem((R + 8, LANES), F32),
            vmem((R, LANES), BF16),
            vmem((R, 2 * LANES), F32),
            *flat,
            vmem((R, 2 * LANES), BF16),
            vmem((R + 8, LANES), F32),
            vmem((8, LANES), F32),
            vmem((NY, 8, LANES), F32),
            vmem((8, LANES), F32),
            vmem((NZ, 8, LANES), F32),
            vmem((8, LANES), F32),
            vmem((8, LANES), F32),
            vmem((NY, NZ, share, LANES), BF16),
            vmem((NY, NZ, share, LANES), BF16),
            vmem((NZ, share, LANES), BF16),
            vmem((NZ, share, LANES), BF16),
            dma((7,)),
            dma((2 * NX,)),
            dma((2 * NX,)),
            dma((2 * NX,)),
            dma((2 * NX,)),
            dma((2,)),
            dma((14,)),
            dma((14,)),
            dma((NY,)),
            dma((NY,)),
            dma((NZ,)),
            dma((NZ,)),
            dma((4, NY)),
            dma((4, NY)),
            dma((NZ,)),
            dma((NZ,)),
        ],
        compiler_params=pltpu.CompilerParams(collective_id=0, has_side_effects=True),
    )(
        tokens, proj_weight, gate_weight, conv_weight, recur_weight, input_weight,
        decay_param.reshape(-1, LANES), out_grad,
    )


def solution(mesh):
    sizes = (16, 8, 4, 2)
    split = Mesh(mesh.devices.reshape(sizes), ("z", "y", "x", "c"))
    span, group = ("z", "y"), ("x", "c")
    placed = (P(span, group), P(None, group), P(None, group), P(), P(), P(), P(), P(span, group))

    def step(*args):
        return per_device((*sizes[:3], args[0].shape[0]), *args)

    return jax.shard_map(
        step,
        mesh=split,
        in_specs=placed,
        out_specs=(P(span, group), P(span, group), P(span, group)),
        check_vma=False,
    )
```

time: 329 us -> 84.1 us (0.26); the launches traced: 323 us -> 83.8 us
  waiting for transfers between devices: 188 us -> 0 us
  Pallas kernels: 0 us -> 80.2 us
  blocking collectives: 69.3 us -> 0 us
  local copies, waits for them, and re-layouts: 20 us -> 2.95 us
  between operations: 15.7 us -> 0.65 us
  matrix products: 14.7 us -> 0 us
  other arithmetic: 10.6 us -> 0 us
  starting transfers between devices: 4.23 us -> 0 us
    reduce_scatter x1 -> x0, waiting for transfers between devices: 83.2 us -> none  [summed_rows(): subtotal = lax.psum_scatter(subtotal, axis, scatter_dimension=0, tiled=True)]
    pallas_call x0 -> x1, Pallas kernels: none -> 80.2 us  [per_device(): pl.pallas_call(functools.partial(kernel, dims), out_shape=(jax.ShapeDtype...]
    all_gather x4 -> x0, blocking collectives: 69.3 us -> none  [collected_together(): both, at, found = (lax.all_gather(jnp.concatenate(lines), axis), 0, {})]
    all_gather x1 -> x0, waiting for transfers between devices: 52.2 us -> none  [per_device(): gathered = lax.all_gather(tokens, 'tp', axis=1, tiled=True)]
    unnamed x4 -> x0, waiting for transfers between devices: 49 us -> none
    dot_general x7 -> x0, matrix products: 14.7 us -> none  [the longest x1 4.18 us: per_device(): jnp.dot(gathered, gate_weight, preferred_element_type=jnp.float32)]
    slice x136 -> x0, local copies, waits for them, and re-layouts: 9.16 us -> none  [the longest x69 6.62 us: per_device(): lax.associative_scan(combine, (shifted, drive_grad), reverse=True, axis=0)]
    pad x68 -> x0, local copies, waits for them, and re-layouts: 7.12 us -> none  [the longest x34 4.81 us: per_device(): lax.associative_scan(combine, (decay_rate, drive), axis=0)]
  transfers between devices with their start and end apart: 5 -> 0, of which waited for: 5 -> 0; matrix products, arithmetic and copies ran while one was open for 0% -> 0% of each run, Pallas kernels for 0% -> 0%
where the time goes in v1:
time: 84.1 us; the launch traced here: 83.8 us
  Pallas kernels  80.2 us (95%)
  local copies, waits for them, and re-layouts  2.95 us (4%)
    pallas_call x1, Pallas kernels, per_device(): pl.pallas_call(functools.partial(kernel, dims), out_shape=(jax.ShapeDtype...  80.2 us
    unnamed x7, local copies, waits for them, and re-layouts  2.95 us

profile of v1, /device:TPU:1, one launch (start us, length us, event | category | flops | bytes accessed | tf_op | source)
XLA Modules:
  0.0 83.8 jit_solution(16171574875768366574)
XLA Ops:
  0.6 80.2 %shard_map.103 = (bf16[768,128]{1,0:T(8,128)(2,1)}, bf16[768,128]{1,0:T(8,128)(2,1)}, f32[16,128]{1,0:T(8,128)}) custom-call(bf16[768,256]{1,0:T(8,128)(2,1)} %tok.1, bf16[2048,128]{1,0:T(8,128)(2,1)} %pw.1, bf16[2048,128]{1,0:T(8,128)(2,1)} %gw.1, f32[4,1024]{1,0:T(4,128)} %cw.1, bf16[16,64,64]{2,1,0:T(8,128)(2,1)} %rw.1, bf16[16,64,64]{2,1,0:T(8,128)(2,1)} %iw.1, ...), custom_call_target="tpu_custom_call" | custom-call | tf_op jit(solution)/shard_map/pallas_call | solution.py:420
  80.9 0.0 copy-start
  80.9 1.7 %copy.14 = bf16[768,128]{1,0:T(8,128)(2,1)} copy(bf16[768,128]{1,0:T(8,128)(2,1)} %get-tuple-element.6) | data formatting | bytes 393216
  82.5 0.0 copy-done
  82.5 0.0 copy-start.1
  82.5 0.7 copy.15
  83.2 0.0 copy-done.1
  83.2 0.6 copy.16
Async XLA Ops:
  80.9 1.7 %copy-start = (bf16[768,128]{1,0:T(8,128)(2,1)S(1)}, bf16[768,128]{1,0:T(8,128)(2,1)}, u32[]{:S(2)}) copy-start(bf16[768,128]{1,0:T(8,128)(2,1)} %get-tuple-element.7) | copy-start | bytes 589828
  82.5 0.7 copy-start.1

commit v2 on v1

--- a/solution.py
+++ b/solution.py
@@ -36,10 +36,10 @@
 
 
 def kernel(
-    dims, tok, pw, gw, cw, rw, iw, dp, og, dproj, dgate, dweight,
+    dims, tok, pw, gw, cw_far, rw, iw, dp_far, og, dproj, dgate, dweight,
     G, WP, WG, OG, RW, IW, ACC, PJ, CV, PRE, A, B, DG, RO, IO, SC, DGL, HP, PP, YN, QN, DR, DC,
-    SUM, RYC, SUMZ, RZC, CF, CB, WS, RY, VZ, RZ,
-    lsem, hps, hpr, hns, hnr, ogs, ags, agr, ycs, ycr, zcs, zcr, rys, ryr, rzs, rzr,
+    GT, SUM, RYC, SUMZ, RZC, CF, CB, WS, RY, VZ, RZ,
+    lsem, hps, hpr, hns, hnr, ogs, ags, agr, ycs, ycr, zcs, zcr, rys, ryr, rzs, rzr, met, cw, dp,
 ):
     NZ, NY, NX, rows = dims
     R = rows + 2 * HALO
@@ -64,6 +64,8 @@
         pltpu.make_async_copy(og, OG.at[pl.ds(HALO, rows)], lsem.at[4]),
         pltpu.make_async_copy(rw.at[pl.ds(2 * tp, 2)], RW, lsem.at[5]),
         pltpu.make_async_copy(iw.at[pl.ds(2 * tp, 2)], IW, lsem.at[6]),
+        pltpu.make_async_copy(cw_far, cw, lsem.at[7]),
+        pltpu.make_async_copy(dp_far, dp, lsem.at[8]),
     ]
     for copy in loads:
         copy.start()
@@ -80,12 +82,25 @@
         for d in range(2):
             greet(z=nz, y=ny, x=k, c=d)
             greet(z=pz, y=py, x=k, c=d)
-    for d in range(1, NY):
+    for d in (1, NY - 1):
         greet(y=lax.rem(y + d, NY))
-    for d in range(1, NZ):
+    for d in (1, NZ - 1):
         greet(z=lax.rem(z + d, NZ))
-    pl.semaphore_wait(barrier, 3 + 4 * NX + NY - 1 + NZ - 1)
-
+    pl.semaphore_wait(barrier, 3 + 4 * NX + 4)
+
+    def tell(sem, **where):
+        pl.semaphore_signal(met.at[sem], inc=1, device_id=where, device_id_type=MESH)
+
+    def tell_y(sem, d):
+        tell(sem, y=lax.rem(y + d, NY))
+        tell(sem, y=lax.rem(y + NY - d, NY))
+
+    def tell_z(sem, d):
+        tell(sem, z=lax.rem(z + d, NZ))
+        tell(sem, z=lax.rem(z + NZ - d, NZ))
+
+    far_y = sorted(range(1, NY), key=lambda d: -min(d, NY - d))
+    far_z = sorted(range(1, NZ), key=lambda d: -min(d, NZ - d))
     pending = []
 
     def send(src, dst, ssem, rsem, **where):
@@ -130,7 +145,9 @@
     give(p1, 7, c=1 - c)
     loads[4].wait()
     send(OG.at[pl.ds(HALO, HALO)], OG.at[pl.ds(HALO + rows, HALO)], ogs.at[0], ogs.at[1], z=pz, y=py)
-    for k in (2, 3, 5, 6):
+    tell_y(0, 1)
+    tell_z(1, 1)
+    for k in (2, 3, 5, 6, 7, 8):
         loads[k].wait()
 
     OG[pl.ds(0, HALO), :] = jnp.zeros((HALO, LANES), BF16)
@@ -174,6 +191,10 @@
         else:
             ACC[...] += out
 
+    pl.semaphore_wait(met.at[0], 2)
+    pl.semaphore_wait(met.at[1], 2)
+    tell_y(2, 2)
+    tell_z(3, 2)
     multiply(p0, p1, True)
     got(piece(x, 1 - c, 0), 6)
     got(piece(x, 1 - c, 1), 7)
@@ -192,6 +213,9 @@
     got(piece(left, 1 - c, 0), 8)
     got(piece(right, 1 - c, 1), 9)
     multiply(piece(left, 1 - c, 0), piece(right, 1 - c, 1))
+    pl.semaphore_wait(met.at[2], 2)
+    pl.semaphore_wait(met.at[3], 2)
+    tell_z(4, 4)
     got(l1, 2)
     give(l1, 10, c=1 - c)
     got(r0, 3)
@@ -200,6 +224,7 @@
     got(piece(left, 1 - c, 1), 10)
     got(piece(right, 1 - c, 0), 11)
     multiply(piece(left, 1 - c, 1), piece(right, 1 - c, 0))
+    pl.semaphore_wait(met.at[4], 2)
     got(o0, 4)
     give(o0, 12, c=1 - c)
     got(o1, 5)
@@ -299,9 +324,15 @@
 
     SUM[...] = nil
     put(SUM, (out_a, out_s, out_c, out_l))
-    for d in range(1, NY):
+    for d in far_y:
         send(SUM, RYC.at[y], ycs.at[d], ycr.at[y], y=lax.rem(y + d, NY))
     RYC[y] = SUM[...]
+
+    def turn(i, _):
+        GT[pl.ds(pl.multiple_of(i * LANES, LANES), LANES), :] = G[i, main, :].T
+        return 0
+
+    lax.fori_loop(0, NZ // 2, turn, 0)
     for d in range(1, NY):
         k = lax.rem(y + d, NY)
         arrived(RYC.at[k], ycs.at[d], ycr.at[k], c=1 - c)
@@ -324,9 +355,10 @@
     total, inside = compose(RYC, NY, y)
     SUMZ[...] = nil
     put(SUMZ, total)
-    for d in range(1, NZ):
+    for d in far_z:
         send(SUMZ, RZC.at[z], zcs.at[d], zcr.at[z], z=lax.rem(z + d, NZ))
     RZC[z] = SUMZ[...]
+    lax.fori_loop(NZ // 2, NZ, turn, 0)
     for d in range(1, NZ):
         k = lax.rem(z + d, NZ)
         arrived(RZC.at[k], zcs.at[d], zcr.at[k], c=1 - c)
@@ -383,10 +415,10 @@
     share = LANES // NY
     per = NZ // 4
     for g in range(4):
-        for i in range(g * per, (g + 1) * per):
-            part = lax.dot_general(G[i, main, :], grad, (((0,), (0,)), ((), ())), preferred_element_type=F32)
-            WS[:, i] = part.astype(BF16).reshape(NY, share, LANES)
-        for d in range(1, NY):
+        part = jnp.dot(GT[pl.ds(g * per * LANES, per * LANES), :], grad, preferred_element_type=F32).astype(BF16)
+        for i in range(per):
+            WS[:, g * per + i] = part[i * LANES : (i + 1) * LANES].reshape(NY, share, LANES)
+        for d in far_y:
             k = lax.rem(y + d, NY)
             send(WS.at[k, pl.ds(g * per, per)], RY.at[y, pl.ds(g * per, per)], rys.at[g, d], ryr.at[g, y], y=k)
     for g in range(4):
@@ -396,7 +428,7 @@
             arrived(RY.at[k, pl.ds(g * per, per)], rys.at[g, d], ryr.at[g, k], c=1 - c)
             total = total + RY[k, pl.ds(g * per, per)].astype(F32)
         VZ[pl.ds(g * per, per)] = total.astype(BF16)
-    for d in range(1, NZ):
+    for d in far_z:
         k = lax.rem(z + d, NZ)
         send(VZ.at[k], RZ.at[z], rzs.at[d], rzr.at[z], z=k)
     total = VZ[z].astype(F32)
@@ -409,6 +441,14 @@
         copy.wait_send()
 
 
+def hand_over(a, b, c, a_out, b_out, c_out, sem):
+    copies = [pltpu.make_async_copy(s, d, sem.at[k]) for k, (s, d) in enumerate(((a, a_out), (b, b_out), (c, c_out)))]
+    for copy in copies:
+        copy.start()
+    for copy in copies:
+        copy.wait()
+
+
 def per_device(dims, tokens, proj_weight, gate_weight, conv_weight, recur_weight, input_weight, decay_param, out_grad):
     NZ, NY, NX, rows = dims
     R = rows + 2 * HALO
@@ -416,15 +456,15 @@
     vmem = pltpu.VMEM
     dma = pltpu.SemaphoreType.DMA
     flat = [vmem((R, LANES), F32)] * 11
-    anywhere, inside = pl.BlockSpec(memory_space=pl.ANY), pl.BlockSpec(memory_space=pltpu.VMEM)
-    return pl.pallas_call(
+    far, anywhere, inside = (pl.BlockSpec(memory_space=m) for m in (pltpu.HBM, pl.ANY, pltpu.VMEM))
+    results = pl.pallas_call(
         functools.partial(kernel, dims),
         out_shape=(
             jax.ShapeDtypeStruct((rows, LANES), BF16),
             jax.ShapeDtypeStruct((rows, LANES), BF16),
             jax.ShapeDtypeStruct((share, LANES), F32),
         ),
-        in_specs=[anywhere, anywhere, anywhere, inside, anywhere, anywhere, inside, anywhere],
+        in_specs=[far] * 8,
         out_specs=(inside, inside, inside),
         scratch_shapes=[
             vmem((4 * NX, R, LANES), BF16),
@@ -440,6 +480,7 @@
             *flat,
             vmem((R, 2 * LANES), BF16),
             vmem((R + 8, LANES), F32),
+            vmem((4 * NX * LANES, rows), BF16),
             vmem((8, LANES), F32),
             vmem((NY, 8, LANES), F32),
             vmem((8, LANES), F32),
@@ -450,7 +491,7 @@
             vmem((NY, NZ, share, LANES), BF16),
             vmem((NZ, share, LANES), BF16),
             vmem((NZ, share, LANES), BF16),
-            dma((7,)),
+            dma((9,)),
             dma((2 * NX,)),
             dma((2 * NX,)),
             dma((2 * NX,)),
@@ -466,12 +507,23 @@
             dma((4, NY)),
             dma((NZ,)),
             dma((NZ,)),
+            pltpu.SemaphoreType.REGULAR((5,)),
+            vmem(conv_weight.shape, F32),
+            vmem((decay_param.shape[0] // LANES, LANES), F32),
         ],
-        compiler_params=pltpu.CompilerParams(collective_id=0, has_side_effects=True),
-    )(
+        compiler_params=pltpu.CompilerParams(collective_id=0, has_side_effects=True, vmem_limit_bytes=40 * 2**20),
+    )(*(pltpu.with_memory_space_constraint(a, pltpu.HBM) for a in (
         tokens, proj_weight, gate_weight, conv_weight, recur_weight, input_weight,
         decay_param.reshape(-1, LANES), out_grad,
-    )
+    )))
+    return pl.pallas_call(
+        hand_over,
+        out_shape=[jax.ShapeDtypeStruct(r.shape, r.dtype) for r in results],
+        in_specs=[inside] * 3,
+        out_specs=[anywhere] * 3,
+        scratch_shapes=[dma((3,))],
+        compiler_params=pltpu.CompilerParams(vmem_limit_bytes=2**21),
+    )(*results)
 
 
 def solution(mesh):

time: 84.1 us -> 78 us (0.927)
  Pallas kernels: 80.2 us -> 76.3 us
  local copies, waits for them, and re-layouts: 2.95 us -> 0 us
    pallas_call x1, Pallas kernels: 80.2 us -> 75.5 us  [per_device(): pl.pallas_call(functools.partial(kernel, dims), out_shape=(jax.ShapeDtype...]
    unnamed x7 -> x0, local copies, waits for them, and re-layouts: 2.95 us -> none
where the time goes in v2:
time: 78 us; the launch traced here: 77 us
  Pallas kernels  76.3 us (98%)
    pallas_call x1, Pallas kernels, per_device(): pl.pallas_call(functools.partial(kernel, dims), out_shape=(jax.ShapeDtype...  75.5 us

profile of v2, /device:TPU:1, one launch (start us, length us, event | category | flops | bytes accessed | tf_op | source)
XLA Modules:
  0.0 77.0 jit_solution(10370454830534094177)
XLA Ops:
  0.6 75.5 %shard_map.103 = (bf16[768,128]{1,0:T(8,128)(2,1)S(1)}, bf16[768,128]{1,0:T(8,128)(2,1)S(1)}, f32[16,128]{1,0:T(8,128)S(1)}) custom-call(bf16[768,256]{1,0:T(8,128)(2,1)} %tok.1, bf16[2048,128]{1,0:T(8,128)(2,1)} %pw.1, bf16[2048,128]{1,0:T(8,128)(2,1)} %gw.1, f32[4,1024]{1,0:T(4,128)} %cw_far.1, bf16[16,64,64]{2,1,0:T(8,128)(2,1)} %rw.1, ...), custom_call_target="tpu_custom_call" | custom-call | tf_op jit(solution)/shard_map/pallas_call | solution.py:460
  76.2 0.8 %shard_map.104 = (bf16[768,128]{1,0:T(8,128)(2,1)}, bf16[768,128]{1,0:T(8,128)(2,1)}, f32[16,128]{1,0:T(8,128)}) custom-call(bf16[768,128]{1,0:T(8,128)(2,1)S(1)} %get-tuple-element.6.a, bf16[768,128]{1,0:T(8,128)(2,1)S(1)} %get-tuple-element.7.b, f32[16,128]{1,0:T(8,128)S(1)} %get-tuple-element.8.c), custom_call_target="tpu_custom_call" | custom-call | tf_op jit(solution)/shard_map/pallas_call | solution.py:519

commit v3 on v2

--- a/solution.py
+++ b/solution.py
@@ -268,7 +268,7 @@
         t = jnp.tanh(GELU_A * (q + GELU_B * (q * q * q)))
         cdf = 0.5 * (1.0 + t)
         DG[at, :] = cot * (q * cdf)
-        DGL[at, :] = cot * (cdf + 0.5 * q * (1.0 - t * t) * (GELU_A * (1.0 + 3.0 * GELU_B * (q * q))))
+        DGL[at, :] = t
         return 0
 
     lax.fori_loop(0, nch, local, 0)
@@ -322,14 +322,32 @@
         for k, value in enumerate(values):
             ref[pl.ds(k, 1), :] = value
 
+    share = LANES // NY
     SUM[...] = nil
     put(SUM, (out_a, out_s, out_c, out_l))
     for d in far_y:
         send(SUM, RYC.at[y], ycs.at[d], ycr.at[y], y=lax.rem(y + d, NY))
     RYC[y] = SUM[...]
 
+    def factors(i, _):
+        at = pl.ds(pl.multiple_of(i * CHUNK, CHUNK), CHUNK)
+        a, ro, io, sc = A[at, :], RO[at, :], IO[at, :], SC[at, :]
+        conv = CV[at, :].astype(F32)
+        q = ACC[at, pl.ds(LANES, LANES)].astype(BF16).astype(F32)
+        t = DGL[at, :]
+        slant = 0.5 * (1.0 + t) + 0.5 * q * (1.0 - t * t) * (GELU_A * (1.0 + 3.0 * GELU_B * (q * q)))
+        DGL[at, :] = OG[at, :].astype(F32) * slant
+        both = sc * io
+        PRE[at, pl.ds(0, LANES)] = (io * conv) * a * a / sc
+        RO[at, :] = slope * ro * (1.0 - ro)
+        IO[at, :] = both
+        SC[at, :] = both * conv * (1.0 - io)
+        return 0
+
+    lax.fori_loop(0, nch, factors, 0)
+
     def turn(i, _):
-        GT[pl.ds(pl.multiple_of(i * LANES, LANES), LANES), :] = G[i, main, :].T
+        GT[:, i] = G[i, main, :].T.reshape(NY, share, rows)
         return 0
 
     lax.fori_loop(0, NZ // 2, turn, 0)
@@ -381,21 +399,14 @@
     def gradients(i, _):
         base = pl.multiple_of(i * CHUNK, CHUNK)
         at = pl.ds(base, CHUNK)
-        a, ro, io, sc = A[at, :], RO[at, :], IO[at, :], SC[at, :]
-        conv = CV[at, :].astype(F32)
-        decayed = a * HP[at, :]
         grad = DG[at, :] + YN[at, :]
-        gated = io * conv
-        DGL[at, :] = DGL[at, :] * (decayed + B[at, :])
-        d_log = grad * (decayed - gated * a * a / sc)
-        DR[at, pl.ds(0, LANES)] = (d_log * slope * ro * (1.0 - ro)).astype(BF16)
-        gs = grad * sc
-        DR[at, pl.ds(LANES, LANES)] = (gs * conv * io * (1.0 - io)).astype(BF16)
-        DC[at, :] = gs * io
+        d_log = grad * (A[at, :] * HP[at, :] - PRE[at, pl.ds(0, LANES)])
+        DR[at, pl.ds(0, LANES)] = (d_log * RO[at, :]).astype(BF16)
+        DR[at, pl.ds(LANES, LANES)] = (grad * SC[at, :]).astype(BF16)
+        DC[at, :] = grad * IO[at, :]
         return 0
 
     lax.fori_loop(0, nch, gradients, 0)
-    dgate[...] = DGL[pl.ds(HALO, rows), :].astype(BF16)
     DC[pl.ds(0, R), :] += lax.dot_general(DR[...], gates, (((1,), (1,)), ((), ())), preferred_element_type=F32)
 
     WIDE = 96
@@ -412,22 +423,58 @@
     lax.fori_loop(0, rows // WIDE, unconvolve, 0)
 
     grad = dproj[...]
-    share = LANES // NY
-    per = NZ // 4
-    for g in range(4):
-        part = jnp.dot(GT[pl.ds(g * per * LANES, per * LANES), :], grad, preferred_element_type=F32).astype(BF16)
-        for i in range(per):
-            WS[:, g * per + i] = part[i * LANES : (i + 1) * LANES].reshape(NY, share, LANES)
-        for d in far_y:
-            k = lax.rem(y + d, NY)
-            send(WS.at[k, pl.ds(g * per, per)], RY.at[y, pl.ds(g * per, per)], rys.at[g, d], ryr.at[g, y], y=k)
-    for g in range(4):
-        total = WS[y, pl.ds(g * per, per)].astype(F32)
-        for d in range(1, NY):
-            k = lax.rem(y + d, NY)
-            arrived(RY.at[k, pl.ds(g * per, per)], rys.at[g, d], ryr.at[g, k], c=1 - c)
-            total = total + RY[k, pl.ds(g * per, per)].astype(F32)
-        VZ[pl.ds(g * per, per)] = total.astype(BF16)
+    half = NZ // 2
+    sides = [pl.ds(0, half), pl.ds(half, half)]
+
+    def along(d):
+        return lax.rem(y + NY + d, NY)
+
+    def partial(d):
+        k = along(d)
+        part = jnp.dot(GT[k].reshape(NZ * share, rows), grad, preferred_element_type=F32)
+        WS[k] = part.astype(BF16).reshape(NZ, share, LANES)
+        return k
+
+    def hop(k, h, slot, d):
+        send(WS.at[k, sides[h]], RY.at[slot, sides[h]], rys.at[slot, h], ryr.at[slot, h], y=along(d))
+
+    def landed(slot, h):
+        arrived(RY.at[slot, sides[h]], rys.at[slot, h], ryr.at[slot, h], c=1 - c)
+
+    def add(k, h, slot):
+        landed(slot, h)
+        WS[k, sides[h]] = (WS[k, sides[h]].astype(F32) + RY[slot, sides[h]].astype(F32)).astype(BF16)
+
+    k = partial(4)
+    hop(k, 0, 0, 2)
+    hop(k, 1, 0, -2)
+    k = partial(3)
+    hop(k, 0, 1, 2)
+    hop(k, 1, 1, 2)
+    k = partial(-3)
+    hop(k, 0, 2, -2)
+    hop(k, 1, 2, -2)
+    hop(partial(2), 1, 3, 2)
+    hop(partial(-2), 0, 4, -2)
+    partial(1)
+    partial(-1)
+    partial(0)
+    dgate[...] = (DGL[pl.ds(HALO, rows), :] * (A[pl.ds(HALO, rows), :] * HP[pl.ds(HALO, rows), :] + B[pl.ds(HALO, rows), :])).astype(BF16)
+    add(along(2), 0, 0)
+    hop(along(2), 0, 3, 2)
+    for h in range(2):
+        add(along(1), h, 1)
+        hop(along(1), h, 5, 1)
+        add(along(-1), h, 2)
+        hop(along(-1), h, 6, -1)
+    add(along(-2), 1, 0)
+    hop(along(-2), 1, 4, -2)
+    for h in range(2):
+        total = WS[y, sides[h]].astype(F32)
+        for slot in (3, 4, 5, 6):
+            landed(slot, h)
+            total = total + RY[slot, sides[h]].astype(F32)
+        VZ[sides[h]] = total.astype(BF16)
     for d in far_z:
         k = lax.rem(z + d, NZ)
         send(VZ.at[k], RZ.at[z], rzs.at[d], rzr.at[z], z=k)
@@ -480,7 +527,7 @@
             *flat,
             vmem((R, 2 * LANES), BF16),
             vmem((R + 8, LANES), F32),
-            vmem((4 * NX * LANES, rows), BF16),
+            vmem((NY, NZ, share, rows), BF16),
             vmem((8, LANES), F32),
             vmem((NY, 8, LANES), F32),
             vmem((8, LANES), F32),
@@ -503,8 +550,8 @@
             dma((NY,)),
             dma((NZ,)),
             dma((NZ,)),
-            dma((4, NY)),
-            dma((4, NY)),
+            dma((7, 2)),
+            dma((7, 2)),
             dma((NZ,)),
             dma((NZ,)),
             pltpu.SemaphoreType.REGULAR((5,)),

time: 78 us -> 75.7 us (0.971)
  the two profiles are of different devices: /device:TPU:1 before, /device:TPU:6 now
where the time goes in v3:
time: 75.7 us; the launch traced here: 75.6 us
  Pallas kernels  74.9 us (99%)
    pallas_call x1, Pallas kernels, per_device(): pl.pallas_call(functools.partial(kernel, dims), out_shape=(jax.ShapeDtype...  74.2 us

profile of v3, /device:TPU:6, one launch (start us, length us, event | category | flops | bytes accessed | tf_op | source)
XLA Modules:
  0.0 75.6 jit_solution(17090179240508317268)
XLA Ops:
  0.6 74.2 %shard_map.103 = (bf16[768,128]{1,0:T(8,128)(2,1)S(1)}, bf16[768,128]{1,0:T(8,128)(2,1)S(1)}, f32[16,128]{1,0:T(8,128)S(1)}) custom-call(bf16[768,256]{1,0:T(8,128)(2,1)} %tok.1, bf16[2048,128]{1,0:T(8,128)(2,1)} %pw.1, bf16[2048,128]{1,0:T(8,128)(2,1)} %gw.1, f32[4,1024]{1,0:T(4,128)} %cw_far.1, bf16[16,64,64]{2,1,0:T(8,128)(2,1)} %rw.1, ...), custom_call_target="tpu_custom_call" | custom-call | tf_op jit(solution)/shard_map/pallas_call | solution.py:507
  74.8 0.8 %shard_map.104 = (bf16[768,128]{1,0:T(8,128)(2,1)}, bf16[768,128]{1,0:T(8,128)(2,1)}, f32[16,128]{1,0:T(8,128)}) custom-call(bf16[768,128]{1,0:T(8,128)(2,1)S(1)} %get-tuple-element.6.a, bf16[768,128]{1,0:T(8,128)(2,1)S(1)} %get-tuple-element.7.b, f32[16,128]{1,0:T(8,128)S(1)} %get-tuple-element.8.c), custom_call_target="tpu_custom_call" | custom-call | tf_op jit(solution)/shard_map/pallas_call | solution.py:566

commit v4 on v3

--- a/solution.py
+++ b/solution.py
@@ -39,7 +39,7 @@
     dims, tok, pw, gw, cw_far, rw, iw, dp_far, og, dproj, dgate, dweight,
     G, WP, WG, OG, RW, IW, ACC, PJ, CV, PRE, A, B, DG, RO, IO, SC, DGL, HP, PP, YN, QN, DR, DC,
     GT, SUM, RYC, SUMZ, RZC, CF, CB, WS, RY, VZ, RZ,
-    lsem, hps, hpr, hns, hnr, ogs, ags, agr, ycs, ycr, zcs, zcr, rys, ryr, rzs, rzr, met, cw, dp,
+    lsem, hys, hyr, hxs, hxr, ogs, ags, agr, ycs, ycr, zcs, zcr, rys, ryr, rzs, rzr, met, cw, dp,
 ):
     NZ, NY, NX, rows = dims
     R = rows + 2 * HALO
@@ -78,15 +78,13 @@
     greet(c=1 - c)
     greet(x=left)
     greet(x=right)
-    for k in range(NX):
-        for d in range(2):
-            greet(z=nz, y=ny, x=k, c=d)
-            greet(z=pz, y=py, x=k, c=d)
+    greet(z=nz, y=ny)
+    greet(z=pz, y=py)
     for d in (1, NY - 1):
         greet(y=lax.rem(y + d, NY))
     for d in (1, NZ - 1):
         greet(z=lax.rem(z + d, NZ))
-    pl.semaphore_wait(barrier, 3 + 4 * NX + 4)
+    pl.semaphore_wait(barrier, 9)
 
     def tell(sem, **where):
         pl.semaphore_signal(met.at[sem], inc=1, device_id=where, device_id_type=MESH)
@@ -119,13 +117,18 @@
     loads[1].wait()
     mine = 2 * tp
     main = pl.ds(HALO, rows)
-    for k in range(NX):
-        for d in range(2):
-            n = 2 * k + d
-            send(G.at[pl.ds(mine, 2), pl.ds(rows, HALO)], G.at[pl.ds(mine, 2), pl.ds(0, HALO)],
-                 hps.at[n], hpr.at[tp], z=nz, y=ny, x=k, c=d)
-            send(G.at[pl.ds(mine, 2), pl.ds(HALO, HALO)], G.at[pl.ds(mine, 2), pl.ds(HALO + rows, HALO)],
-                 hns.at[n], hnr.at[tp], z=pz, y=py, x=k, c=d)
+    edges = (pl.ds(0, HALO), pl.ds(HALO + rows, HALO))
+    send(G.at[pl.ds(mine, 2), pl.ds(rows, HALO)], G.at[pl.ds(mine, 2), edges[0]], hys.at[0], hyr.at[0], z=nz, y=ny)
+    send(G.at[pl.ds(mine, 2), pl.ds(HALO, HALO)], G.at[pl.ds(mine, 2), edges[1]], hys.at[1], hyr.at[1], z=pz, y=py)
+
+    def halo(xx, cc, k):
+        return G.at[pl.ds(4 * xx + 2 * cc, 2), edges[k]]
+
+    def pass_halo(xx, slot, k, **where):
+        send(halo(xx, c, k), halo(xx, c, k), hxs.at[slot, k], hxr.at[slot, k], **where)
+
+    def got_halo(xx, cc, slot, k):
+        arrived(halo(xx, cc, k), hxs.at[slot, k], hxr.at[slot, k], c=1 - c)
 
     def piece(xx, cc, h):
         return 4 * xx + 2 * cc + h
@@ -139,8 +142,6 @@
     p0, p1 = piece(x, c, 0), piece(x, c, 1)
     give(p0, 0, x=right)
     give(p1, 1, x=left)
-    give(p1, 2, x=right)
-    give(p0, 3, x=left)
     give(p0, 6, c=1 - c)
     give(p1, 7, c=1 - c)
     loads[4].wait()
@@ -164,18 +165,17 @@
         axis=0,
     )
 
-    for n in range(2 * NX):
-        arrived(G.at[pl.ds(2 * n, 2), pl.ds(0, HALO)], hps.at[n], hpr.at[n], c=1 - c)
-        arrived(G.at[pl.ds(2 * n, 2), pl.ds(HALO + rows, HALO)], hns.at[n], hnr.at[n], c=1 - c)
+    for k in range(2):
+        arrived(halo(x, c, k), hys.at[k], hyr.at[k], c=1 - c)
+        pass_halo(x, 0, k, x=right)
+        pass_halo(x, 1, k, x=left)
+        pass_halo(x, 3, k, c=1 - c)
+    give(p1, 2, x=right)
+    give(p0, 3, x=left)
     arrived(OG.at[pl.ds(HALO + rows, HALO)], ogs.at[0], ogs.at[1], c=1 - c)
-
-    @pl.when(sp == 0)
-    def _():
-        G[:, pl.ds(0, HALO), :] = jnp.zeros((4 * NX, HALO, LANES), BF16)
 
     @pl.when(sp == nsp - 1)
     def _():
-        G[:, pl.ds(HALO + rows, HALO), :] = jnp.zeros((4 * NX, HALO, LANES), BF16)
         OG[pl.ds(HALO + rows, HALO), :] = jnp.zeros((HALO, LANES), BF16)
 
     def multiply(i0, i1, first=False):
@@ -198,20 +198,34 @@
     multiply(p0, p1, True)
     got(piece(x, 1 - c, 0), 6)
     got(piece(x, 1 - c, 1), 7)
+    for k in range(2):
+        got_halo(x, 1 - c, 3, k)
     multiply(piece(x, 1 - c, 0), piece(x, 1 - c, 1))
 
     l0, l1 = piece(left, c, 0), piece(left, c, 1)
     r0, r1 = piece(right, c, 0), piece(right, c, 1)
     o0, o1 = piece(opp, c, 0), piece(opp, c, 1)
     got(l0, 0)
+    for k in range(2):
+        got_halo(left, c, 0, k)
+    pass_halo(left, 2, 0, x=right)
     give(l0, 4, x=right)
     give(l0, 8, c=1 - c)
     got(r1, 1)
+    for k in range(2):
+        got_halo(right, c, 1, k)
+    pass_halo(right, 2, 1, x=left)
     give(r1, 5, x=left)
     give(r1, 9, c=1 - c)
+    for k in range(2):
+        pass_halo(left, 4, k, c=1 - c)
+        pass_halo(right, 5, k, c=1 - c)
     multiply(l0, r1)
     got(piece(left, 1 - c, 0), 8)
     got(piece(right, 1 - c, 1), 9)
+    for k in range(2):
+        got_halo(left, 1 - c, 4, k)
+        got_halo(right, 1 - c, 5, k)
     multiply(piece(left, 1 - c, 0), piece(right, 1 - c, 1))
     pl.semaphore_wait(met.at[2], 2)
     pl.semaphore_wait(met.at[3], 2)
@@ -225,6 +239,9 @@
     got(piece(right, 1 - c, 0), 11)
     multiply(piece(left, 1 - c, 1), piece(right, 1 - c, 0))
     pl.semaphore_wait(met.at[4], 2)
+    for k in range(2):
+        got_halo(opp, c, 2, k)
+        pass_halo(opp, 6, k, c=1 - c)
     got(o0, 4)
     give(o0, 12, c=1 - c)
     got(o1, 5)
@@ -232,9 +249,15 @@
     multiply(o0, o1)
     got(piece(opp, 1 - c, 0), 12)
     got(piece(opp, 1 - c, 1), 13)
+    for k in range(2):
+        got_halo(opp, 1 - c, 6, k)
     multiply(piece(opp, 1 - c, 0), piece(opp, 1 - c, 1))
 
     PJ[pl.ds(8, R), :] = ACC[:, pl.ds(0, LANES)].astype(BF16).astype(F32)
+
+    @pl.when(sp == 0)
+    def _():
+        PJ[pl.ds(8, HALO), :] = jnp.zeros((HALO, LANES), F32)
 
     def convolve(i, _):
         base = pl.multiple_of(i * CHUNK, CHUNK)
@@ -539,10 +562,10 @@
             vmem((NZ, share, LANES), BF16),
             vmem((NZ, share, LANES), BF16),
             dma((9,)),
-            dma((2 * NX,)),
-            dma((2 * NX,)),
-            dma((2 * NX,)),
-            dma((2 * NX,)),
+            dma((2,)),
+            dma((2,)),
+            dma((7, 2)),
+            dma((7, 2)),
             dma((2,)),
             dma((14,)),
             dma((14,)),

time: 75.7 us -> 73.4 us (0.970)
  the two profiles are of different devices: /device:TPU:6 before, /device:TPU:1 now
where the time goes in v4:
time: 73.4 us; the launch traced here: 73.3 us
  Pallas kernels  72.7 us (99%)
    pallas_call x1, Pallas kernels, per_device(): pl.pallas_call(functools.partial(kernel, dims), out_shape=(jax.ShapeDtype...  71.9 us

profile of v4, /device:TPU:1, one launch (start us, length us, event | category | flops | bytes accessed | tf_op | source)
XLA Modules:
  0.0 73.3 jit_solution(853107049358742495)
XLA Ops:
  0.6 71.9 %shard_map.103 = (bf16[768,128]{1,0:T(8,128)(2,1)S(1)}, bf16[768,128]{1,0:T(8,128)(2,1)S(1)}, f32[16,128]{1,0:T(8,128)S(1)}) custom-call(bf16[768,256]{1,0:T(8,128)(2,1)} %tok.1, bf16[2048,128]{1,0:T(8,128)(2,1)} %pw.1, bf16[2048,128]{1,0:T(8,128)(2,1)} %gw.1, f32[4,1024]{1,0:T(4,128)} %cw_far.1, bf16[16,64,64]{2,1,0:T(8,128)(2,1)} %rw.1, ...), custom_call_target="tpu_custom_call" | custom-call | tf_op jit(solution)/shard_map/pallas_call | solution.py:530
  72.5 0.8 %shard_map.104 = (bf16[768,128]{1,0:T(8,128)(2,1)}, bf16[768,128]{1,0:T(8,128)(2,1)}, f32[16,128]{1,0:T(8,128)}) custom-call(bf16[768,128]{1,0:T(8,128)(2,1)S(1)} %get-tuple-element.6.a, bf16[768,128]{1,0:T(8,128)(2,1)S(1)} %get-tuple-element.7.b, f32[16,128]{1,0:T(8,128)S(1)} %get-tuple-element.8.c), custom_call_target="tpu_custom_call" | custom-call | tf_op jit(solution)/shard_map/pallas_call | solution.py:589

commit v5 on v4

--- a/solution.py
+++ b/solution.py
@@ -485,13 +485,13 @@
     dgate[...] = (DGL[pl.ds(HALO, rows), :] * (A[pl.ds(HALO, rows), :] * HP[pl.ds(HALO, rows), :] + B[pl.ds(HALO, rows), :])).astype(BF16)
     add(along(2), 0, 0)
     hop(along(2), 0, 3, 2)
+    add(along(-2), 1, 0)
+    hop(along(-2), 1, 4, -2)
     for h in range(2):
         add(along(1), h, 1)
         hop(along(1), h, 5, 1)
         add(along(-1), h, 2)
         hop(along(-1), h, 6, -1)
-    add(along(-2), 1, 0)
-    hop(along(-2), 1, 4, -2)
     for h in range(2):
         total = WS[y, sides[h]].astype(F32)
         for slot in (3, 4, 5, 6):

time: 73.4 us -> 73.3 us (level)
  no operation moved by 1% of the time
where the time goes in v5:
time: 73.3 us; the launch traced here: 72.6 us
  Pallas kernels  72 us (98%)
    pallas_call x1, Pallas kernels, per_device(): pl.pallas_call(functools.partial(kernel, dims), out_shape=(jax.ShapeDtype...  71.2 us

profile of v5, /device:TPU:1, one launch (start us, length us, event | category | flops | bytes accessed | tf_op | source)
XLA Modules:
  0.0 72.6 jit_solution(5833998370090594428)
XLA Ops:
  0.6 71.2 %shard_map.103 = (bf16[768,128]{1,0:T(8,128)(2,1)S(1)}, bf16[768,128]{1,0:T(8,128)(2,1)S(1)}, f32[16,128]{1,0:T(8,128)S(1)}) custom-call(bf16[768,256]{1,0:T(8,128)(2,1)} %tok.1, bf16[2048,128]{1,0:T(8,128)(2,1)} %pw.1, bf16[2048,128]{1,0:T(8,128)(2,1)} %gw.1, f32[4,1024]{1,0:T(4,128)} %cw_far.1, bf16[16,64,64]{2,1,0:T(8,128)(2,1)} %rw.1, ...), custom_call_target="tpu_custom_call" | custom-call | tf_op jit(solution)/shard_map/pallas_call | solution.py:530
  71.8 0.8 %shard_map.104 = (bf16[768,128]{1,0:T(8,128)(2,1)}, bf16[768,128]{1,0:T(8,128)(2,1)}, f32[16,128]{1,0:T(8,128)}) custom-call(bf16[768,128]{1,0:T(8,128)(2,1)S(1)} %get-tuple-element.6.a, bf16[768,128]{1,0:T(8,128)(2,1)S(1)} %get-tuple-element.7.b, f32[16,128]{1,0:T(8,128)S(1)} %get-tuple-element.8.c), custom_call_target="tpu_custom_call" | custom-call | tf_op jit(solution)/shard_map/pallas_call | solution.py:589
